TPU v7x, 32 devices: a whole 2x2x4 slice. The times are simulated.
32 devices in a mesh: ep: 8 (over z, x), tp: 4 (over y, core).
Axes of the slice: x: 2, y: 2, z: 4, core: 2. Of those that a mesh axis runs over, the one named last changes fastest.
Arguments:
- tokens: bfloat16 [4096, 2048], P(('ep', 'tp')), may hold values from -6 to 6
- expert_ids: int32 [4096, 4], P('ep'), may hold values from 0 to 7, all different within a row; in each aligned block of 128 rows (0 to 127, 128 to 255, ...) at most 64 rows name the same one
- gate_values: float32 [4096, 4], P('ep'), may hold values from 0.1 to 1
- norm_gain: float32 [2048], replicated, may hold values from 0.1 to 1.9
- gate_weight: bfloat16 [8, 2048, 1024], P('ep', None, 'tp'), may hold values from -0.125 to 0.125
- up_weight: bfloat16 [8, 2048, 1024], P('ep', None, 'tp'), may hold values from -0.125 to 0.125
- down_weight: bfloat16 [8, 1024, 2048], P('ep', 'tp'), may hold values from -0.1875 to 0.1875
- out_gain: float32 [2048], P('tp'), may hold values from 0.1 to 1.9
Outputs:
- mixed: bfloat16 [4096, 2048], P('ep', 'tp')
Inputs may be any that keep to these rules, and one draw needn't show every extreme that they name: `expert_ids`: each row names 4 different experts of 0 to 7; within the rows of one device (aligned blocks of 128 rows) no expert is named more than 64 times, and in some blocks one expert is named exactly 64 times.
All inputs are finite; a program needn't handle non-finite values.
Results may differ from a plain program's by a relative error of at most 0.0025.
Values may be sent and summed in bfloat16 or wider, within the bound.
A program may use at most 64 MiB of HBM per device.

v0:
```python
import jax
import jax.numpy as jnp
from jax import lax
from jax.sharding import PartitionSpec as P

epsilon = 1e-05
clamp_limit = 7.0
sigmoid_alpha = 1.702


def taken_in(shard, axis, dim, absorb, state):
    everything = jax.tree.map(lambda a: lax.all_gather(a, axis, axis=dim, tiled=True), shard)
    return absorb(state, everything, jnp.int32(0))


def rms_rows(values, gain):
    mean_sq = jnp.mean(values * values, axis=-1, keepdims=True)
    return values * lax.rsqrt(mean_sq + epsilon) * gain


def clamped_unit(gate_part, up_part):
    glu_part = jnp.minimum(gate_part, clamp_limit)
    lin_part = jnp.clip(up_part, -clamp_limit, clamp_limit)
    return glu_part * jax.nn.sigmoid(sigmoid_alpha * glu_part) * (lin_part + 1.0)


def local(
    tokens, expert_ids, gate_values, norm_gain, gate_weight, up_weight, down_weight, out_gain
):
    expert_groups = lax.axis_size("ep")
    width_groups = lax.axis_size("tp")
    tok_rows = tokens.shape[0]
    model_width = tokens.shape[1]
    top_count = expert_ids.shape[1]
    capacity = tok_rows // 2
    per_rank = capacity // width_groups
    slice_w = model_width // width_groups
    normed = rms_rows(tokens.astype(jnp.float32), norm_gain).astype(jnp.bfloat16)
    blocks = expert_ids.reshape(width_groups, tok_rows * top_count)
    onehot = (
        blocks[:, :, None] == jnp.arange(expert_groups, dtype=jnp.int32)[None, None, :]
    ).astype(jnp.int32)
    slot_num = jnp.sum((jnp.cumsum(onehot, axis=1) - onehot) * onehot, axis=2)
    own_rank = lax.axis_index("tp")
    own_ids = lax.dynamic_index_in_dim(blocks, own_rank, 0, keepdims=False)
    own_slots = lax.dynamic_index_in_dim(slot_num, own_rank, 0, keepdims=False)
    target = own_ids * capacity + own_slots
    entry_token = jnp.arange(tok_rows * top_count, dtype=jnp.int32) // top_count
    owner_row = (
        jnp.full((expert_groups * capacity,), tok_rows, jnp.int32).at[target].set(entry_token)
    )
    padded = jnp.concatenate([normed, jnp.zeros((1, model_width), jnp.bfloat16)], axis=0)
    outgoing = padded[owner_row].reshape(expert_groups * width_groups, per_rank, model_width)
    arrived = lax.all_to_all(outgoing, ("ep", "tp"), split_axis=0, concat_axis=0, tiled=True)
    arrived_rows = arrived.reshape(-1, model_width)
    row_total = arrived_rows.shape[0]
    hidden_width = gate_weight.shape[2] * width_groups
    blank_acts = jnp.zeros((row_total, hidden_width), jnp.bfloat16)

    def add_hidden(activated, pieces, offset):
        gate_part = jnp.dot(arrived_rows, pieces[0][0], preferred_element_type=jnp.float32)
        up_part = jnp.dot(arrived_rows, pieces[1][0], preferred_element_type=jnp.float32)
        fresh = clamped_unit(gate_part, up_part).astype(jnp.bfloat16)
        return lax.dynamic_update_slice_in_dim(activated, fresh, offset, 1)

    activated = taken_in((gate_weight, up_weight), "tp", 2, add_hidden, blank_acts)

    def add_output(running, w_piece, offset):
        act_part = lax.dynamic_slice_in_dim(activated, offset, w_piece.shape[1], 1)
        return running + jnp.dot(act_part, w_piece[0], preferred_element_type=jnp.float32)

    blank_out = jnp.zeros((row_total, model_width), jnp.float32)
    result = taken_in(down_weight, "tp", 1, add_output, blank_out).astype(jnp.bfloat16)
    outbound = result.reshape(expert_groups, width_groups, per_rank, width_groups, slice_w)
    outbound = outbound.transpose(0, 3, 1, 2, 4)
    landed = lax.all_to_all(
        outbound.reshape(expert_groups * width_groups, width_groups, per_rank, slice_w),
        ("ep", "tp"),
        split_axis=0,
        concat_axis=0,
        tiled=True,
    )
    returned = landed.reshape(-1, slice_w)
    rank_part = slot_num // per_rank
    within = slot_num % per_rank
    source_col = jnp.arange(width_groups, dtype=jnp.int32)[:, None]
    row_index = (
        (blocks * width_groups + rank_part) * width_groups + source_col
    ) * per_rank + within
    picked = returned[row_index.reshape(-1)].astype(jnp.float32)
    picked = picked.reshape(width_groups * tok_rows, top_count, slice_w)
    combined = jnp.sum(gate_values[:, :, None] * picked, axis=1)
    local_sq = jnp.sum(combined * combined, axis=1)
    total_sq = lax.psum(local_sq, "tp")
    row_scale = lax.rsqrt(total_sq / model_width + epsilon)
    return (combined * row_scale[:, None] * out_gain).astype(jnp.bfloat16)


def solution(mesh):
    in_specs = (
        P(("ep", "tp"), None),
        P("ep", None),
        P("ep", None),
        P(),
        P("ep", None, "tp"),
        P("ep", None, "tp"),
        P("ep", "tp", None),
        P("tp"),
    )
    out_specs = P("ep", "tp")
    return jax.shard_map(local, mesh=mesh, in_specs=in_specs, out_specs=out_specs, check_vma=False)
```

profile of v0, /device:TPU:17, one launch (start us, length us, event | category | flops | bytes accessed | tf_op | source)
XLA Modules:
  0.0 236.1 jit_solution(15095314450109095855)
XLA Ops:
  6.5 0.0 copy-start.2
  6.5 0.0 copy-start.1
  6.5 0.0 all-gather.6.cloned.1.call-start
  6.5 0.7 all-gather.6.cloned.1.call-update
  7.3 0.0 copy-start.3
  7.3 0.0 all-gather.4.cloned.1.call-start
  7.3 0.7 all-gather.4.cloned.1.call-update
  8.0 0.0 all-gather.8.cloned.1.call-start
  8.1 0.7 all-gather.8.cloned.1.call-update
  8.8 0.0 copy-done.2
  8.8 0.1 copy.11
  8.9 0.2 eq.28
  9.1 4.5 %reduce-window.6 = s32[4,8,4,128]{3,1,2,0:T(8,128)S(1)} reduce-window(s32[4,8,4,128]{3,1,2,0:T(8,128)S(1)} %fusion.18, s32[]{:T(128)} %constant.77.clone.1), window={size=1x1x1x128 pad=0_0x0_0x0_0x127_0}, to_apply=%region_1.0 | reduce-window | flops 2080768 | bytes 131076 | tf_op jit(solution)/shard_map/reduce-window
  13.6 0.4 slice_reduce_fusion
  14.1 0.2 reshape.220
  14.3 0.0 copy-done.1
  14.3 0.2 fusion.11
  14.5 0.0 copy-done.3
  14.5 0.2 fusion.13
  14.7 0.1 fusion.17
  14.9 2.4 %scatter_custom_fusion = s32[512]{0:T(512)S(1)} fusion(s32[512]{0:T(512)S(1)} %bitcast.53, s32[512]{0:T(512)S(1)} %add_select_fusion, s32[]{:T(128)} %constant.75.clone.1), kind=kCustom, calls=%fused_computation.47 | custom fusion | bytes 2052 | tf_op jit(solution)/shard_map/scatter | solution.py:50
  17.3 2.5 %gather_fusion = bf16[512,2048]{1,0:T(8,128)(2,1)S(1)} fusion(bf16[129,2048]{1,0:T(8,128)(2,1)S(1)} %concatenate.3, s32[1024]{0:T(1024)S(1)} %pad_clamp_fusion), kind=kCustom, calls=%fused_computation | custom fusion | bytes 4196352 | tf_op jit(solution)/shard_map/gather | solution.py:53
  19.8 54.5 %all_to_all.10 = bf16[32,16,2048]{2,1,0:T(8,128)(2,1)} all-to-all(bf16[32,16,2048]{2,1,0:T(8,128)(2,1)S(1)} %bitcast.45), channel_id=1, replica_groups=mesh['ep'=8,'tp'=4] {'ep','tp'}, dimensions={0} | all-to-all | bytes 4194304 | tf_op jit(solution)/shard_map/all_to_all | solution.py:54
  74.3 0.0 all-gather.6.cloned.1.call-done
  74.3 0.0 copy-start
  74.3 6.7 %fusion.2 = f32[512,1024]{1,0:T(8,128)} fusion(bf16[512,2048]{1,0:T(8,128)(2,1)} %bitcast.47, bf16[1,2048,1024]{2,1,0:T(8,128)(2,1)} %all-gather.6.cloned.1.call-done), kind=kOutput, calls=%fused_computation.5 | convolution fusion | flops 2147483648 | bytes 8388608 | tf_op jit(solution)/shard_map/dot_general | solution.py:62
  81.0 19.9 %all-gather.4.cloned.1.call-done = bf16[1,2048,1024]{2,1,0:T(8,128)(2,1)} async-done(((bf16[1,2048,256]{2,1,0:T(8,128)(2,1)}), bf16[1,2048,1024]{2,1,0:T(8,128)(2,1)}) %all-gather.4.cloned.1.call-update) | async-done | bytes 4194320 | tf_op jit(solution)/shard_map/all_gather | solution.py:12
  100.9 35.9 %all-gather.8.cloned.1.call-done = bf16[1,1024,2048]{2,1,0:T(8,128)(2,1)} async-done(((bf16[1,256,2048]{2,1,0:T(8,128)(2,1)}), bf16[1,1024,2048]{2,1,0:T(8,128)(2,1)}) %all-gather.8.cloned.1.call-update) | async-done | bytes 4194320 | tf_op jit(solution)/shard_map/all_gather | solution.py:12
  136.8 0.0 copy-done
  136.8 10.4 %fusion.6 = bf16[512,2048]{1,0:T(8,128)(2,1)} fusion(bf16[1,1024,2048]{2,1,0:T(8,128)(2,1)} %all-gather.8.cloned.1.call-done, f32[512,1024]{1,0:T(8,128)} %fusion.2, bf16[512,2048]{1,0:T(8,128)(2,1)S(1)} %bitcast.48, bf16[1,2048,1024]{2,1,0:T(8,128)(2,1)} %all-gather.4.cloned.1.call-done), kind=kOutput, calls=%fused_computation.10 | convolution fusion | flops 4301258752 | bytes 14680064 | tf_op jit(solution)/shard_map/dot_general | solution.py:70
  147.3 3.3 %reshape.224 = bf16[8,4,16,4,512]{4,3,2,1,0:T(4,128)(2,1)S(1)} reshape(bf16[512,2048]{1,0:T(8,128)(2,1)} %fusion.6) | data formatting | bytes 4194304 | tf_op jit(solution)/shard_map/reshape | solution.py:74
  150.6 1.9 copy.13
  152.5 0.0 copy-start.4
  152.5 4.8 %all-to-all-start.1 = ((bf16[32,4,16,512]{3,2,1,0:T(8,128)(2,1)}), bf16[32,4,16,512]{3,2,1,0:T(8,128)(2,1)S(1)}, u32[]{:S(2)}, u32[]{:S(2)}) async-start(bf16[32,4,16,512]{3,2,1,0:T(8,128)(2,1)} %bitcast.46), calls=%async_computation.1 | async-start | bytes 4194304 | tf_op jit(solution)/shard_map/all_to_all | solution.py:76
  157.3 0.1 copy.14
  157.4 0.2 mul.126
  157.6 0.0 copy-done.4
  157.6 0.1 copy.10
  157.8 0.1 compare_select_fusion
  157.9 46.7 %all-to-all-done.1 = bf16[32,4,16,512]{3,2,1,0:T(8,128)(2,1)S(1)} async-done(((bf16[32,4,16,512]{3,2,1,0:T(8,128)(2,1)}), bf16[32,4,16,512]{3,2,1,0:T(8,128)(2,1)S(1)}, u32[]{:S(2)}, u32[]{:S(2)}) %all-to-all-start.1) | async-done | bytes 2097184 | tf_op jit(solution)/shard_map/all_to_all | solution.py:76
  204.6 9.2 %gather_fusion.1 = bf16[2048,512]{1,0:T(8,128)(2,1)} fusion(bf16[2048,512]{1,0:T(8,128)(2,1)S(1)} %bitcast.44, s32[2048]{0:T(1024)S(1)} %broadcast_clamp_fusion), kind=kCustom, calls=%fused_computation.1 | custom fusion | bytes 4202496 | tf_op jit(solution)/shard_map/gather | solution.py:90
  213.8 4.8 %reshape.227 = f32[512,4,512]{2,1,0:T(4,128)} reshape(bf16[2048,512]{1,0:T(8,128)(2,1)} %gather_fusion.1) | data formatting | bytes 6291456 | tf_op jit(solution)/shard_map/convert_element_type | solution.py:90
  218.5 0.0 copy-start.5
  218.5 4.8 %multiply_reduce_fusion = f32[512,512]{1,0:T(8,128)S(1)} fusion(f32[512,4,512]{2,1,0:T(4,128)} %reshape.227, f32[512,4]{1,0:T(8,128)S(1)} %copy.10), kind=kLoop, calls=%fused_computation.9 | loop fusion | flops 1835008 | bytes 5251072 | tf_op jit(solution)/shard_map/reduce_sum | solution.py:92
  223.3 0.1 multiply_reduce_fusion.1
  223.5 5.1 %psum.7 = f32[512]{0:T(512)S(1)} all-reduce(f32[512]{0:T(512)S(1)} %multiply_reduce_fusion.1), channel_id=1, replica_groups=mesh['ep'=8,'tp'=4] {'tp'}, use_global_device_ids=true, to_apply=%region_7.8 | all-reduce | flops 512 | bytes 4096 | tf_op jit(solution)/shard_map/psum | solution.py:94
  228.6 0.0 copy-done.5
  228.6 1.0 multiply_convert_fusion.1
  (15 shorter events, 0.2 us)
Async XLA Ops:
  6.5 2.2 copy-start.2
  6.5 7.7 %copy-start.1 = (bf16[128,2048]{1,0:T(8,128)(2,1)S(1)}, bf16[128,2048]{1,0:T(8,128)(2,1)}, u32[]{:S(2)}) copy-start(bf16[128,2048]{1,0:T(8,128)(2,1)} %param.8) | copy-start | bytes 1572868
  6.5 67.8 %all-gather.6.cloned.1.call-start = ((), (), s32[]{:S(2)}) async-start(), calls=%async_computation.3 | async-start | bytes 5242880 | tf_op jit(solution)/shard_map/all_gather | solution.py:12
  7.3 7.2 %copy-start.3 = (f32[2048]{0:T(1024)S(1)}, f32[2048]{0:T(1024)}, u32[]{:S(2)}) copy-start(f32[2048]{0:T(1024)} %param.11) | copy-start | bytes 24580
  7.3 93.6 %all-gather.4.cloned.1.call-start = ((), (), s32[]{:S(2)}) async-start(), calls=%async_computation.2 | async-start | bytes 5242880 | tf_op jit(solution)/shard_map/all_gather | solution.py:12
  8.0 128.8 %all-gather.8.cloned.1.call-start = ((), (), s32[]{:S(2)}) async-start(), calls=%async_computation.4 | async-start | bytes 5242880 | tf_op jit(solution)/shard_map/all_gather | solution.py:12
  74.3 62.5 %copy-start = (bf16[32,16,2048]{2,1,0:T(8,128)(2,1)S(1)}, bf16[32,16,2048]{2,1,0:T(8,128)(2,1)}, u32[]{:S(2)}) copy-start(bf16[32,16,2048]{2,1,0:T(8,128)(2,1)} %all_to_all.10) | copy-start | bytes 6291460
  152.5 5.2 %copy-start.4 = (f32[512,4]{0,1:T(4,128)S(1)}, f32[512,4]{0,1:T(4,128)}, u32[]{:S(2)}) copy-start(f32[512,4]{0,1:T(4,128)} %param.10) | copy-start | bytes 24580
  152.5 52.1 %all-to-all-start.1 = ((bf16[32,4,16,512]{3,2,1,0:T(8,128)(2,1)}), bf16[32,4,16,512]{3,2,1,0:T(8,128)(2,1)S(1)}, u32[]{:S(2)}, u32[]{:S(2)}) async-start(bf16[32,4,16,512]{3,2,1,0:T(8,128)(2,1)} %bitcast.46), calls=%async_computation.1 | async-start | bytes 4194304 | tf_op jit(solution)/shard_map/all_to_all | solution.py:76
  218.5 10.1 %copy-start.5 = (f32[512]{0:T(512)S(1)}, f32[512]{0:T(512)}, u32[]{:S(2)}) copy-start(f32[512]{0:T(512)} %param.15) | copy-start | bytes 6148
Sparse Core Ops, SparseCore 0:
  8.9 55.3 all-gather.5
  65.8 35.0 all-gather.3
  102.5 34.3 all-gather.7
where the time goes:
time: 240 us; the launch traced here: 236 us
  waiting for transfers between devices  105 us (44%)
  blocking collectives  59.6 us (25%)
  local copies, waits for them, and re-layouts  25.5 us (11%)
  matrix products  17.1 us (7%)
  between operations  13.3 us (6%)
  other arithmetic  11.1 us (5%)
  starting transfers between devices  4.83 us (2%)
    all_gather x3, waiting for transfers between devices, taken_in(): lax.all_gather(a, axis, axis=dim, tiled=True)  55.9 us
    all_to_all x1, blocking collectives, local(): lax.all_to_all(outgoing, ('ep', 'tp'), split_axis=0, concat_axis=0, tiled...  54.5 us
    all_to_all x1, waiting for transfers between devices, local(): lax.all_to_all(outbound.reshape(expert_groups * width_groups, width_group...  46.7 us
    dot_general x1, matrix products, add_output(): jnp.dot(act_part, w_piece[0], preferred_element_type=jnp.float32)  10.4 us
    gather x1, local copies, waits for them, and re-layouts, local(): picked = returned[row_index.reshape(-1)].astype(jnp.float32)  9.17 us
    dot_general x1, matrix products, add_hidden(): jnp.dot(arrived_rows, pieces[1][0], preferred_element_type=jnp.float32)  6.66 us
    reshape x2, local copies, waits for them, and re-layouts, local(): result.reshape(expert_groups, width_groups, per_rank, width_groups, slice_w)  5.2 us
    psum x1, blocking collectives, local(): total_sq = lax.psum(local_sq, 'tp')  5.12 us
  transfers between devices with their start and end apart: 4, of which 3 were waited for; matrix products, arithmetic and copies ran while one was open for 8% of the time, Pallas kernels for 0%

commit v1 on v0

v1 whole, which is shorter than its diff:
```python
import functools

import jax
import jax.numpy as jnp
from jax import lax
from jax.experimental import pallas as pl
from jax.experimental.pallas import tpu as pltpu
from jax.sharding import PartitionSpec as P

epsilon = 1e-05
clamp_limit = 7.0
sigmoid_alpha = 1.702
F32 = jnp.float32
BF16 = jnp.bfloat16
MESH = pl.DeviceIdType.MESH


def clamped_unit(gate_part, up_part):
    glu_part = jnp.minimum(gate_part, clamp_limit)
    lin_part = jnp.clip(up_part, -clamp_limit, clamp_limit)
    return glu_part * jax.nn.sigmoid(sigmoid_alpha * glu_part) * (lin_part + 1.0)


def kernel(
    n_ep, n_tp,
    tokens_ref, ids_ref, values_ref, gain_ref, gate_hbm, up_hbm, down_hbm, out_gain_ref,
    mixed_ref,
    gate_all, up_all, down_all, gain_all, normed, pick, outgoing, arrived, acts, results,
    returned, combined, final,
    local_sem, gain_send, gain_recv, w_send, w_fwd, w_recv,
    d_send, d_recv, r_send, r_recv, f_send, f_recv,
):
    me = lax.axis_index("ep")
    rank = lax.axis_index("tp")
    core = lax.rem(rank, 2)
    side = lax.div(rank, 2)
    sides = n_tp // 2
    sibling = rank + 1 - 2 * core
    toks, width = tokens_ref.shape
    top = ids_ref.shape[1]
    cap = toks // 2
    part = gate_all.shape[2]
    slice_w = width // n_tp
    rows = n_ep * cap
    chunks = 2 + n_tp

    def across(d):
        return lax.rem(side + d, sides) * 2 + core

    def across_sibling(d):
        return lax.rem(side + d, sides) * 2 + 1 - core

    def ep_peer(d):
        return lax.rem(me + d, n_ep)

    def tp_peer(d):
        return lax.rem(rank + d, n_tp)

    own_copies = [
        pltpu.make_async_copy(gate_hbm.at[0], gate_all.at[rank], local_sem.at[0]),
        pltpu.make_async_copy(up_hbm.at[0], up_all.at[rank], local_sem.at[1]),
    ]
    for q in range(n_tp):
        own_copies.append(
            pltpu.make_async_copy(
                down_hbm.at[0, :, pl.ds(q * slice_w, slice_w)],
                down_all.at[q, rank],
                local_sem.at[2 + q],
            )
        )
    for copy in own_copies:
        copy.start()

    barrier = pltpu.get_barrier_semaphore()
    for d in range(1, n_ep):
        pl.semaphore_signal(
            barrier, inc=1, device_id={"ep": ep_peer(d), "tp": rank}, device_id_type=MESH
        )
    for d in range(1, n_tp):
        pl.semaphore_signal(
            barrier, inc=1, device_id={"ep": me, "tp": tp_peer(d)}, device_id_type=MESH
        )
    pl.semaphore_wait(barrier, n_ep - 1 + n_tp - 1)

    def piece(chunk, slot):
        if chunk == 0:
            return gate_all.at[slot]
        if chunk == 1:
            return up_all.at[slot]
        return down_all.at[chunk - 2, slot]

    def weight_copy(chunk, slot, sem, to):
        return pltpu.make_async_remote_copy(
            src_ref=piece(chunk, slot), dst_ref=piece(chunk, slot),
            send_sem=sem, recv_sem=w_recv.at[chunk, slot],
            device_id={"ep": me, "tp": to}, device_id_type=MESH,
        )

    sends = []
    for chunk in range(chunks):
        own_copies[chunk].wait()
        for d in range(1, sides):
            sends.append(weight_copy(chunk, rank, w_send.at[chunk, d], across(d)))
            sends[-1].start()
        sends.append(weight_copy(chunk, rank, w_send.at[chunk, 0], sibling))
        sends[-1].start()

    gain_all[rank] = out_gain_ref[...]

    step = 16

    def norm_rows(i, carry):
        at = pl.ds(pl.multiple_of(i * step, step), step)
        x = tokens_ref[at, :].astype(F32)
        mean_sq = jnp.mean(x * x, axis=-1, keepdims=True)
        normed[at, :] = (x * lax.rsqrt(mean_sq + epsilon) * gain_ref[...]).astype(BF16)
        return carry

    lax.fori_loop(0, toks // step, norm_rows, 0)

    block = pl.ds(pl.multiple_of(rank * toks, toks), toks)
    ids = ids_ref[block, :]
    values = values_ref[block, :]
    lane = lax.broadcasted_iota(jnp.int32, (toks, 128), 1)
    named = [ids[:, k:k + 1] == lane for k in range(top)]
    member = sum(jnp.where(m, 1.0, 0.0) for m in named).astype(BF16)
    row_i = lax.broadcasted_iota(jnp.int32, (toks, toks), 0)
    col_i = lax.broadcasted_iota(jnp.int32, (toks, toks), 1)
    lower = jnp.where(col_i < row_i, 1.0, 0.0).astype(BF16)
    earlier = jnp.dot(lower, member, preferred_element_type=F32)
    entry = lax.broadcasted_iota(jnp.int32, (toks, rows), 1).astype(F32)
    onehot = jnp.zeros((toks, rows), F32)
    weight = jnp.zeros((toks, rows), F32)
    for k in range(top):
        slot = jnp.sum(jnp.where(named[k], earlier, 0.0), axis=1, keepdims=True)
        target = ids[:, k:k + 1].astype(F32) * cap + slot
        hit = entry == target
        onehot = onehot + jnp.where(hit, 1.0, 0.0)
        weight = weight + jnp.where(hit, values[:, k:k + 1], 0.0)
    pick[...] = jnp.transpose(onehot).astype(BF16)

    def dispatch_rows(e, carry):
        at = pl.ds(pl.multiple_of(e * cap, cap), cap)
        for n in range(width // 512):
            outgoing[e, :, n * 512:(n + 1) * 512] = jnp.dot(
                pick[at, :], normed[:, n * 512:(n + 1) * 512], preferred_element_type=F32
            ).astype(BF16)
        return carry

    lax.fori_loop(0, n_ep, dispatch_rows, 0)
    arrived[me] = outgoing[me]

    def dispatch_copy(d):
        return pltpu.make_async_remote_copy(
            src_ref=outgoing.at[ep_peer(d)], dst_ref=arrived.at[me],
            send_sem=d_send.at[d], recv_sem=d_recv.at[me],
            device_id={"ep": ep_peer(d), "tp": rank}, device_id_type=MESH,
        )

    for d in range(1, n_ep):
        sends.append(dispatch_copy(d))
        sends[-1].start()

    def gain_copy(d):
        return pltpu.make_async_remote_copy(
            src_ref=gain_all.at[rank], dst_ref=gain_all.at[rank],
            send_sem=gain_send.at[d], recv_sem=gain_recv.at[rank],
            device_id={"ep": me, "tp": tp_peer(d)}, device_id_type=MESH,
        )

    for d in range(1, n_tp):
        sends.append(gain_copy(d))
        sends[-1].start()

    def got(ref, sem):
        pltpu.make_async_copy(ref, ref, sem).wait()

    def relay(chunk):
        for d in range(1, sides):
            slot = across(d)
            got(piece(chunk, slot), w_recv.at[chunk, slot])
            sends.append(weight_copy(chunk, slot, w_fwd.at[chunk, d], sibling))
            sends[-1].start()

    tile_e = 2

    def hidden(slot):
        def tile(i, carry):
            at = pl.ds(i * tile_e, tile_e)
            x = arrived[at].reshape(tile_e * cap, width)
            g = jnp.dot(x, gate_all[slot], preferred_element_type=F32)
            u = jnp.dot(x, up_all[slot], preferred_element_type=F32)
            acts[slot, pl.ds(pl.multiple_of(i * tile_e * cap, tile_e * cap), tile_e * cap), :] = (
                clamped_unit(g, u).astype(BF16)
            )
            return carry

        lax.fori_loop(0, n_ep // tile_e, tile, 0)

    relay(0)
    for d in range(1, n_ep):
        src = ep_peer(d)
        got(arrived.at[src], d_recv.at[src])
    hidden(rank)
    for chunk in range(2):
        got(piece(chunk, sibling), w_recv.at[chunk, sibling])
    hidden(sibling)
    relay(1)
    for d in range(1, sides):
        hidden(across(d))
    for d in range(1, sides):
        slot = across_sibling(d)
        for chunk in range(2):
            got(piece(chunk, slot), w_recv.at[chunk, slot])
        hidden(slot)

    def return_copy(q, d):
        return pltpu.make_async_remote_copy(
            src_ref=results.at[q, ep_peer(d)], dst_ref=returned.at[q, me],
            send_sem=r_send.at[q, d], recv_sem=r_recv.at[q, me],
            device_id={"ep": ep_peer(d), "tp": rank}, device_id_type=MESH,
        )

    for q in range(n_tp):
        relay(2 + q)
        got(piece(2 + q, sibling), w_recv.at[2 + q, sibling])
        for d in range(1, sides):
            slot = across_sibling(d)
            got(piece(2 + q, slot), w_recv.at[2 + q, slot])

        def tile(i, carry):
            at = pl.ds(pl.multiple_of(i * tile_e * cap, tile_e * cap), tile_e * cap)
            total = jnp.zeros((tile_e * cap, slice_w), F32)
            for s in range(n_tp):
                total = total + jnp.dot(acts[s, at, :], down_all[q, s], preferred_element_type=F32)
            results[q, pl.ds(i * tile_e, tile_e)] = total.astype(BF16).reshape(tile_e, cap, slice_w)
            return carry

        lax.fori_loop(0, n_ep // tile_e, tile, 0)
        for d in range(1, n_ep):
            sends.append(return_copy(q, d))
            sends[-1].start()
        returned[q, me] = results[q, me]

    high = weight.astype(BF16)
    rest = weight - high.astype(F32)
    mid = rest.astype(BF16)
    low = (rest - mid.astype(F32)).astype(BF16)
    total_sq = jnp.zeros((toks, 1), F32)
    for q in range(n_tp):
        for d in range(1, n_ep):
            src = ep_peer(d)
            got(returned.at[q, src], r_recv.at[q, src])
        values_in = returned[q].reshape(rows, slice_w)
        both = jnp.dot(low, values_in, preferred_element_type=F32)
        both = both + jnp.dot(mid, values_in, preferred_element_type=F32)
        both = both + jnp.dot(high, values_in, preferred_element_type=F32)
        combined[q] = both
        total_sq = total_sq + jnp.sum(both * both, axis=1, keepdims=True)
    row_scale = lax.rsqrt(total_sq / width + epsilon)
    for d in range(1, n_tp):
        src = tp_peer(d)
        got(gain_all.at[src], gain_recv.at[src])
    for q in range(n_tp):
        final[q] = (combined[q] * row_scale * gain_all[q]).astype(BF16)

    def final_copy(d):
        return pltpu.make_async_remote_copy(
            src_ref=final.at[tp_peer(d)], dst_ref=mixed_ref.at[block, :],
            send_sem=f_send.at[d], recv_sem=f_recv.at[rank],
            device_id={"ep": me, "tp": tp_peer(d)}, device_id_type=MESH,
        )

    for d in range(1, n_tp):
        sends.append(final_copy(d))
        sends[-1].start()
    mixed_ref[block, :] = final[rank]
    for d in range(1, n_tp):
        src = tp_peer(d)
        there = mixed_ref.at[pl.ds(pl.multiple_of(src * toks, toks), toks), :]
        got(there, f_recv.at[src])
    for copy in sends:
        copy.wait_send()


def local(
    tokens, expert_ids, gate_values, norm_gain, gate_weight, up_weight, down_weight, out_gain
):
    n_ep = lax.axis_size("ep")
    n_tp = lax.axis_size("tp")
    toks, width = tokens.shape
    cap = toks // 2
    rows = n_ep * cap
    part = gate_weight.shape[2]
    slice_w = width // n_tp
    chunks = 2 + n_tp
    sides = n_tp // 2
    vmem = pl.BlockSpec(memory_space=pltpu.VMEM)
    hbm = pl.BlockSpec(memory_space=pl.ANY)
    dma = pltpu.SemaphoreType.DMA
    return pl.pallas_call(
        functools.partial(kernel, n_ep, n_tp),
        out_shape=jax.ShapeDtypeStruct((n_tp * toks, slice_w), BF16),
        in_specs=[vmem, vmem, vmem, vmem, hbm, hbm, hbm, vmem],
        out_specs=vmem,
        scratch_shapes=[
            pltpu.VMEM((n_tp, width, part), BF16),
            pltpu.VMEM((n_tp, width, part), BF16),
            pltpu.VMEM((n_tp, n_tp, part, slice_w), BF16),
            pltpu.VMEM((n_tp, 1, slice_w), F32),
            pltpu.VMEM((toks, width), BF16),
            pltpu.VMEM((rows, toks), BF16),
            pltpu.VMEM((n_ep, cap, width), BF16),
            pltpu.VMEM((n_ep, cap, width), BF16),
            pltpu.VMEM((n_tp, rows, part), BF16),
            pltpu.VMEM((n_tp, n_ep, cap, slice_w), BF16),
            pltpu.VMEM((n_tp, n_ep, cap, slice_w), BF16),
            pltpu.VMEM((n_tp, toks, slice_w), F32),
            pltpu.VMEM((n_tp, toks, slice_w), BF16),
            dma((chunks,)),
            dma((n_tp,)),
            dma((n_tp,)),
            dma((chunks, sides)),
            dma((chunks, sides)),
            dma((chunks, n_tp)),
            dma((n_ep,)),
            dma((n_ep,)),
            dma((n_tp, n_ep)),
            dma((n_tp, n_ep)),
            dma((n_tp,)),
            dma((n_tp,)),
        ],
        compiler_params=pltpu.CompilerParams(
            collective_id=0, has_side_effects=True, vmem_limit_bytes=60 * 1024 * 1024
        ),
    )(
        tokens, expert_ids, gate_values, norm_gain.reshape(1, width),
        gate_weight, up_weight, down_weight, out_gain.reshape(1, slice_w),
    )


def solution(mesh):
    in_specs = (
        P(("ep", "tp"), None),
        P("ep", None),
        P("ep", None),
        P(),
        P("ep", None, "tp"),
        P("ep", None, "tp"),
        P("ep", "tp", None),
        P("tp"),
    )
    out_specs = P("ep", "tp")
    return jax.shard_map(local, mesh=mesh, in_specs=in_specs, out_specs=out_specs, check_vma=False)
```

time: 240 us -> 125 us (0.52)
  the two profiles are of different devices: /device:TPU:17 before, /device:TPU:31 now
where the time goes in v1:
time: 125 us
  Pallas kernels  120 us (96%)
  local copies, waits for them, and re-layouts  4.29 us (3%)
    pallas_call x1, Pallas kernels, local(): pl.pallas_call(functools.partial(kernel, n_ep, n_tp), out_shape=jax.Shape...  120 us
    unnamed x5, local copies, waits for them, and re-layouts  4.29 us

profile of v1, /device:TPU:31, one launch (start us, length us, event | category | flops | bytes accessed | tf_op | source)
XLA Modules:
  0.0 124.6 jit_solution(2105588735344564555)
XLA Ops:
  0.0 0.0 copy-start
  0.0 1.6 %copy.9.ids_ref = s32[512,4]{1,0:T(8,128)} copy(s32[512,4]{0,1:T(4,128)} %param.9) | data formatting | bytes 16384 | tf_op args[1]
  1.6 0.0 copy-done
  1.6 0.9 copy.10.values_ref
  2.4 120.3 %shard_map.82 = bf16[512,512]{1,0:T(8,128)(2,1)} custom-call(bf16[128,2048]{1,0:T(8,128)(2,1)} %tokens_ref.1, s32[512,4]{1,0:T(8,128)} %copy.9.ids_ref, f32[512,4]{1,0:T(8,128)} %copy.10.values_ref, f32[1,2048]{1,0:T(1,128)} %bitcast.2, bf16[1,2048,256]{2,1,0:T(8,128)(2,1)} %gate_hbm.1, bf16[1,2048,256]{2,1,0:T(8,128)(2,1)} %up_hbm.1, ...), custom_call_target="tpu_custom_call" | custom-call | tf_op jit(solution)/shard_map/pallas_call | solution.py:301
  122.7 1.9 %copy.12 = bf16[512,512]{1,0:T(8,128)(2,1)} copy(bf16[512,512]{1,0:T(8,128)(2,1)} %shard_map.82) | data formatting | bytes 1048576
Async XLA Ops:
  0.0 1.6 %copy-start = (f32[512,4]{0,1:T(4,128)S(1)}, f32[512,4]{0,1:T(4,128)}, u32[]{:S(2)}) copy-start(f32[512,4]{0,1:T(4,128)} %param.10) | copy-start | bytes 24580

commit v2 on v1

--- a/solution.py
+++ b/solution.py
@@ -37,7 +37,7 @@
     sides = n_tp // 2
     sibling = rank + 1 - 2 * core
     toks, width = tokens_ref.shape
-    top = ids_ref.shape[1]
+    top = ids_ref.shape[0]
     cap = toks // 2
     part = gate_all.shape[2]
     slice_w = width // n_tp
@@ -49,6 +49,11 @@
 
     def across_sibling(d):
         return lax.rem(side + d, sides) * 2 + 1 - core
+
+    far_first = sorted(range(1, n_ep), key=lambda d: (abs(2 * d - n_ep), d))
+
+    def ep_source(d):
+        return lax.rem(me + n_ep - d, n_ep)
 
     def ep_peer(d):
         return lax.rem(me + d, n_ep)
@@ -119,9 +124,11 @@
     lax.fori_loop(0, toks // step, norm_rows, 0)
 
     block = pl.ds(pl.multiple_of(rank * toks, toks), toks)
-    ids = ids_ref[block, :]
-    values = values_ref[block, :]
-    lane = lax.broadcasted_iota(jnp.int32, (toks, 128), 1)
+    both_t = jnp.concatenate([ids_ref[:, block].astype(F32), values_ref[:, block]], axis=0)
+    both = jnp.transpose(both_t)
+    ids = both[:, :top]
+    values = both[:, top:]
+    lane = lax.broadcasted_iota(jnp.int32, (toks, 128), 1).astype(F32)
     named = [ids[:, k:k + 1] == lane for k in range(top)]
     member = sum(jnp.where(m, 1.0, 0.0) for m in named).astype(BF16)
     row_i = lax.broadcasted_iota(jnp.int32, (toks, toks), 0)
@@ -133,7 +140,7 @@
     weight = jnp.zeros((toks, rows), F32)
     for k in range(top):
         slot = jnp.sum(jnp.where(named[k], earlier, 0.0), axis=1, keepdims=True)
-        target = ids[:, k:k + 1].astype(F32) * cap + slot
+        target = ids[:, k:k + 1] * cap + slot
         hit = entry == target
         onehot = onehot + jnp.where(hit, 1.0, 0.0)
         weight = weight + jnp.where(hit, values[:, k:k + 1], 0.0)
@@ -157,7 +164,7 @@
             device_id={"ep": ep_peer(d), "tp": rank}, device_id_type=MESH,
         )
 
-    for d in range(1, n_ep):
+    for d in far_first:
         sends.append(dispatch_copy(d))
         sends[-1].start()
 
@@ -197,17 +204,29 @@
 
         lax.fori_loop(0, n_ep // tile_e, tile, 0)
 
-    relay(0)
-    for d in range(1, n_ep):
-        src = ep_peer(d)
-        got(arrived.at[src], d_recv.at[src])
-    hidden(rank)
+    def hidden_block(slots, src):
+        x = arrived[src]
+        for slot in slots:
+            g = jnp.dot(x, gate_all[slot], preferred_element_type=F32)
+            u = jnp.dot(x, up_all[slot], preferred_element_type=F32)
+            acts[slot, pl.ds(pl.multiple_of(src * cap, cap), cap), :] = (
+                clamped_unit(g, u).astype(BF16)
+            )
+
     for chunk in range(2):
         got(piece(chunk, sibling), w_recv.at[chunk, sibling])
-    hidden(sibling)
-    relay(1)
+    hidden_block([rank, sibling], me)
+    for i, d in enumerate(far_first):
+        if i == n_ep // 2 - 1:
+            relay(0)
+        if i == n_ep - 2:
+            relay(1)
+        src = ep_source(d)
+        got(arrived.at[src], d_recv.at[src])
+        hidden_block([rank, sibling], src)
     for d in range(1, sides):
         hidden(across(d))
+    relay(2)
     for d in range(1, sides):
         slot = across_sibling(d)
         for chunk in range(2):
@@ -222,7 +241,8 @@
         )
 
     for q in range(n_tp):
-        relay(2 + q)
+        if q > 0:
+            relay(2 + q)
         got(piece(2 + q, sibling), w_recv.at[2 + q, sibling])
         for d in range(1, sides):
             slot = across_sibling(d)
@@ -237,7 +257,7 @@
             return carry
 
         lax.fori_loop(0, n_ep // tile_e, tile, 0)
-        for d in range(1, n_ep):
+        for d in far_first:
             sends.append(return_copy(q, d))
             sends[-1].start()
         returned[q, me] = results[q, me]
@@ -334,7 +354,7 @@
             collective_id=0, has_side_effects=True, vmem_limit_bytes=60 * 1024 * 1024
         ),
     )(
-        tokens, expert_ids, gate_values, norm_gain.reshape(1, width),
+        tokens, expert_ids.T, gate_values.T, norm_gain.reshape(1, width),
         gate_weight, up_weight, down_weight, out_gain.reshape(1, slice_w),
     )
 

time: 125 us -> 121 us (0.968)
  the two profiles are of different devices: /device:TPU:31 before, /device:TPU:17 now
where the time goes in v2:
time: 121 us
  Pallas kernels  119 us (98%)
  local copies, waits for them, and re-layouts  1.87 us (2%)
    pallas_call x1, Pallas kernels, local(): pl.pallas_call(functools.partial(kernel, n_ep, n_tp), out_shape=jax.Shape...  119 us

profile of v2, /device:TPU:17, one launch (start us, length us, event | category | flops | bytes accessed | tf_op | source)
XLA Modules:
  0.0 120.7 jit_solution(17507546213966708665)
XLA Ops:
  0.0 118.8 %shard_map.82 = bf16[512,512]{1,0:T(8,128)(2,1)} custom-call(bf16[128,2048]{1,0:T(8,128)(2,1)} %tokens_ref.1, s32[4,512]{1,0:T(4,128)} %bitcast.4, f32[4,512]{1,0:T(4,128)} %bitcast.5, f32[1,2048]{1,0:T(1,128)} %bitcast.6, bf16[1,2048,256]{2,1,0:T(8,128)(2,1)} %gate_hbm.1, bf16[1,2048,256]{2,1,0:T(8,128)(2,1)} %up_hbm.1, bf16[1,256,2048]{2,1,0:T(8,128)(2,1)} %down_hbm.1, ...), custom_call_target="tpu_custom_call" | custom-call | tf_op jit(solution)/shard_map/pallas_call | solution.py:321
  118.8 1.9 %copy.10 = bf16[512,512]{1,0:T(8,128)(2,1)} copy(bf16[512,512]{1,0:T(8,128)(2,1)} %shard_map.82) | data formatting | bytes 1048576

commit v3 on v2

--- a/solution.py
+++ b/solution.py
@@ -146,16 +146,12 @@
         weight = weight + jnp.where(hit, values[:, k:k + 1], 0.0)
     pick[...] = jnp.transpose(onehot).astype(BF16)
 
-    def dispatch_rows(e, carry):
+    def dispatch_rows(e):
         at = pl.ds(pl.multiple_of(e * cap, cap), cap)
         for n in range(width // 512):
             outgoing[e, :, n * 512:(n + 1) * 512] = jnp.dot(
                 pick[at, :], normed[:, n * 512:(n + 1) * 512], preferred_element_type=F32
             ).astype(BF16)
-        return carry
-
-    lax.fori_loop(0, n_ep, dispatch_rows, 0)
-    arrived[me] = outgoing[me]
 
     def dispatch_copy(d):
         return pltpu.make_async_remote_copy(
@@ -164,9 +160,12 @@
             device_id={"ep": ep_peer(d), "tp": rank}, device_id_type=MESH,
         )
 
-    for d in far_first:
-        sends.append(dispatch_copy(d))
-        sends[-1].start()
+    for i, d in enumerate(far_first + [0]):
+        dispatch_rows(ep_peer(d))
+        if i > 0:
+            sends.append(dispatch_copy(far_first[i - 1]))
+            sends[-1].start()
+    arrived[me] = outgoing[me]
 
     def gain_copy(d):
         return pltpu.make_async_remote_copy(

time: 121 us -> 120 us (level)
  no operation moved by 1% of the time
where the time goes in v3:
time: 120 us
  Pallas kernels  118 us (98%)
  local copies, waits for them, and re-layouts  1.87 us (2%)
    pallas_call x1, Pallas kernels, local(): pl.pallas_call(functools.partial(kernel, n_ep, n_tp), out_shape=jax.Shape...  118 us

profile of v3, /device:TPU:17, one launch (start us, length us, event | category | flops | bytes accessed | tf_op | source)
XLA Modules:
  0.0 120.3 jit_solution(12225589534457111555)
XLA Ops:
  0.0 118.4 %shard_map.82 = bf16[512,512]{1,0:T(8,128)(2,1)} custom-call(bf16[128,2048]{1,0:T(8,128)(2,1)} %tokens_ref.1, s32[4,512]{1,0:T(4,128)} %bitcast.4, f32[4,512]{1,0:T(4,128)} %bitcast.5, f32[1,2048]{1,0:T(1,128)} %bitcast.6, bf16[1,2048,256]{2,1,0:T(8,128)(2,1)} %gate_hbm.1, bf16[1,2048,256]{2,1,0:T(8,128)(2,1)} %up_hbm.1, bf16[1,256,2048]{2,1,0:T(8,128)(2,1)} %down_hbm.1, ...), custom_call_target="tpu_custom_call" | custom-call | tf_op jit(solution)/shard_map/pallas_call | solution.py:320
  118.4 1.9 %copy.10 = bf16[512,512]{1,0:T(8,128)(2,1)} copy(bf16[512,512]{1,0:T(8,128)(2,1)} %shard_map.82) | data formatting | bytes 1048576
